TPU v7x, 512 devices: a whole 4x8x8 slice. The times are simulated.
512 devices in a mesh: sp: 64 (over z, y), tp: 8 (over x, core).
Axes of the slice: x: 4, y: 8, z: 8, core: 2. Of those that a mesh axis runs over, the one named last changes fastest.
Arguments:
- latent_tokens: bfloat16 [8192, 2048], P(('sp', 'tp')), may hold values from -6 to 6
- context_tokens: bfloat16 [512, 2048], P('sp'), may hold values from -6 to 6
- cond: float32 [2048], replicated, may hold values from -6 to 6
- ctx_cond: float32 [2048], replicated, may hold values from -6 to 6
- mod_shift: bfloat16 [2048, 2048], P('sp', 'tp'), may hold values from -0.125 to 0.125
- mod_scale: bfloat16 [2048, 2048], P('sp', 'tp'), may hold values from -0.125 to 0.125
- mod_gate: bfloat16 [2048, 2048], P('sp', 'tp'), may hold values from -0.125 to 0.125
- norm_gain: float32 [2048], replicated, may hold values from 0.1 to 1.9
- w_query: bfloat16 [2048, 1536], P(None, 'tp'), may hold values from -0.125 to 0.125
- query_gain: float32 [96], replicated, may hold values from 0.8 to 2
- w_down_kv: bfloat16 [2048, 256], replicated, may hold values from -0.125 to 0.125
- w_rope_key: bfloat16 [2048, 32], replicated, may hold values from -0.125 to 0.125
- kv_gain: float32 [256], replicated, may hold values from 0.1 to 1.9
- w_up_kv: bfloat16 [2, 256, 1024], P(None, None, 'tp'), may hold values from -0.375 to 0.375
- key_gain: float32 [96], replicated, may hold values from 0.8 to 2
- ctx_lift: float32 [16], P('tp'), may hold values from 1.5 to 220
- w_output: bfloat16 [1024, 2048], P('tp'), may hold values from -0.1875 to 0.1875
Outputs:
- updated: bfloat16 [8192, 2048], P(('sp', 'tp'))
All inputs are finite; a program needn't handle non-finite values.
Results may differ from a plain program's by a relative error of at most 0.007.
Values may be sent and summed in bfloat16 or wider, within the bound.
A program may use at most 64 MiB of HBM per device.

v0:
```python
import functools
import jax
import jax.numpy as jnp
from jax import lax
from jax.sharding import Mesh
from jax.sharding import PartitionSpec as P

HD = 64
ROPE = 32
QK = 96
GRID_W = 64
SP = ("sp_0", "sp_1")
SP_TP = ("sp_0", "sp_1", "tp")
EPS = 1e-06
THETA = 10000.0


def over_axes(value, axes):
    return functools.reduce(lax.psum, axes, value)


def in_one_piece(arrays, axis, dim, along):
    ends, at = ([], 0)
    for a in arrays[:-1]:
        at += a.shape[along]
        ends.append(at)
    both = jnp.concatenate(arrays, axis=along)
    return tuple(jnp.split(lax.all_gather(both, axis, axis=dim, tiled=True), ends, axis=along))


def copy_for_each(value, axis):
    copies = jnp.broadcast_to(value, (lax.axis_size(axis), *value.shape))
    return lax.all_to_all(copies, axis, split_axis=0, concat_axis=0, tiled=True)


def joined_along(tiles, dim):
    tiles = jnp.moveaxis(tiles, 0, dim)
    shape = tiles.shape
    return tiles.reshape(*shape[:dim], shape[dim] * shape[dim + 1], *shape[dim + 2 :])


def collect(value, axis, dim):
    tiles = copy_for_each(value, axis)
    return joined_along(tiles, dim)


def split_up(value, dim, count):
    shape = value.shape
    tiles = value.reshape(*shape[:dim], count, shape[dim] // count, *shape[dim + 1 :])
    return jnp.moveaxis(tiles, dim, 0)


def sent_and_summed(value, axis, dim):
    count = lax.axis_size(axis)
    tiles = lax.all_to_all(split_up(value, dim, count), axis, 0, 0, tiled=True)
    return jnp.sum(tiles.astype(jnp.float32), axis=0)


def rms_normed(values, gain_vector):
    values = values.astype(jnp.float32)
    inv_root = lax.rsqrt(jnp.mean(values * values, axis=-1, keepdims=True) + EPS)
    return values * inv_root * gain_vector


def grid_angles(position, width):
    freq_count = width // 4
    inverse = THETA ** (-jnp.arange(freq_count, dtype=jnp.float32) / freq_count)
    row_index = (position // GRID_W).astype(jnp.float32)
    col_index = (position % GRID_W).astype(jnp.float32)
    return jnp.concatenate([row_index[:, None] * inverse, col_index[:, None] * inverse], axis=-1)


def rotate_tail(head_rows, angle, plain):
    tail = head_rows[..., plain:]
    half_width = tail.shape[-1] // 2
    cosine = jnp.cos(angle)[:, None, :]
    sine_val = jnp.sin(angle)[:, None, :]
    front_half = tail[..., :half_width]
    back_half = tail[..., half_width:]
    return jnp.concatenate(
        [
            head_rows[..., :plain],
            front_half * cosine - back_half * sine_val,
            back_half * cosine + front_half * sine_val,
        ],
        axis=-1,
    )


def modulation(signal, weight):
    return jnp.dot(signal, weight.astype(jnp.float32))


def compress(hidden, w_down_kv, w_rope_key, kv_gain):
    latent = rms_normed(jnp.dot(hidden, w_down_kv, preferred_element_type=jnp.float32), kv_gain)
    rope_key = jnp.dot(hidden, w_rope_key, preferred_element_type=jnp.float32)
    return (latent.astype(jnp.bfloat16), rope_key.astype(jnp.bfloat16))


def expand(latent, rope_key, w_up_kv, key_gain, angle):
    row_count = latent.shape[0]
    head_count = w_up_kv.shape[2] // HD
    key_plain = jnp.dot(latent, w_up_kv[0], preferred_element_type=jnp.float32).reshape(
        row_count, head_count, HD
    )
    shared = jnp.broadcast_to(
        rope_key.astype(jnp.float32)[:, None, :], (row_count, head_count, ROPE)
    )
    keys = rms_normed(jnp.concatenate([key_plain, shared], axis=-1), key_gain)
    if angle is not None:
        keys = rotate_tail(keys, angle, HD)
    values = jnp.dot(latent, w_up_kv[1], preferred_element_type=jnp.float32).astype(jnp.bfloat16)
    return (keys.astype(jnp.bfloat16), values.reshape(row_count, head_count, HD))


def absorb(carry, query_heads, keys, values, lift):
    highest, total, mixed = carry
    scores = (
        jnp.einsum("qhd,khd->hqk", query_heads, keys, preferred_element_type=jnp.float32)
        * QK ** (-0.5)
        + lift
    )
    new_high = jnp.maximum(highest, jnp.max(scores, axis=-1))
    weights = jnp.exp(scores - new_high[:, :, None])
    factor = jnp.exp(highest - new_high)
    total = total * factor + jnp.sum(weights, axis=-1)
    update = jnp.einsum(
        "hqk,khd->qhd", weights.astype(jnp.bfloat16), values, preferred_element_type=jnp.float32
    )
    mixed = mixed * jnp.transpose(factor)[:, :, None] + update
    return (new_high, total, mixed)


def local(
    latent_tokens,
    context_tokens,
    cond,
    ctx_cond,
    mod_shift,
    mod_scale,
    mod_gate,
    norm_gain,
    w_query,
    query_gain,
    w_down_kv,
    w_rope_key,
    kv_gain,
    w_up_kv,
    key_gain,
    ctx_lift,
    w_output,
):
    tp_count = lax.axis_size("tp")
    sp_index = lax.axis_index(SP)
    piece_rows = mod_shift.shape[0]
    own_start = sp_index * piece_rows
    lat_signal = jax.nn.silu(lax.dynamic_slice_in_dim(cond, own_start, piece_rows, 0))
    ctx_signal = jax.nn.silu(lax.dynamic_slice_in_dim(ctx_cond, own_start, piece_rows, 0))
    both_signal = jnp.stack([lat_signal, ctx_signal])
    shift_part = modulation(both_signal, mod_shift)
    scale_part = modulation(both_signal, mod_scale)
    gate_part = modulation(lat_signal[None, :], mod_gate)
    shift_sum, scale_sum, gate_sum = (
        over_axes(shift_part, SP),
        over_axes(scale_part, SP),
        over_axes(gate_part, SP),
    )
    shift_vec, scale_vec, gate_vec = in_one_piece((shift_sum, scale_sum, gate_sum), "tp", 1, 0)
    hidden_lat = (
        rms_normed(latent_tokens, norm_gain) * (1.0 + scale_vec[0]) + shift_vec[0]
    ).astype(jnp.bfloat16)
    ctx_rows = lax.all_gather(context_tokens, SP, axis=0, tiled=True)
    ctx_hidden = (rms_normed(ctx_rows, norm_gain) * (1.0 + scale_vec[1]) + shift_vec[1]).astype(
        jnp.bfloat16
    )
    ctx_latent, ctx_rope = compress(ctx_hidden, w_down_kv, w_rope_key, kv_gain)
    ctx_keys, ctx_values = expand(ctx_latent, ctx_rope, w_up_kv, key_gain, None)
    head_count = ctx_lift.shape[0]
    local_rows = latent_tokens.shape[0]
    group_rows = local_rows * tp_count
    group_start = sp_index * group_rows
    qk_width = head_count * QK
    piece = collect(hidden_lat, "tp", 0)
    row_count = piece.shape[0]
    position = group_start + jnp.arange(row_count, dtype=jnp.int32)
    latent, rope_key = compress(piece, w_down_kv, w_rope_key, kv_gain)
    keys, values = expand(latent, rope_key, w_up_kv, key_gain, grid_angles(position, ROPE))
    make_row_count = piece.shape[0]
    position = group_start + jnp.arange(make_row_count, dtype=jnp.int32)
    raw = jnp.dot(piece, w_query, preferred_element_type=jnp.float32).reshape(
        make_row_count, head_count, QK
    )
    turned = rotate_tail(rms_normed(raw, query_gain), grid_angles(position, ROPE), HD)
    projected = jnp.concatenate(
        [
            turned.astype(jnp.bfloat16).reshape(make_row_count, qk_width),
            keys.reshape(row_count, qk_width),
            values.reshape(row_count, head_count * HD),
        ],
        axis=1,
    )
    queries = projected[:, :qk_width]
    group_keys = projected[:, qk_width : 2 * qk_width]
    group_values = projected[:, 2 * qk_width :]
    query_heads = queries.reshape(group_rows, head_count, QK)
    start_carry = (
        jnp.full((head_count, group_rows), -1e30, jnp.float32),
        jnp.zeros((head_count, group_rows), jnp.float32),
        jnp.zeros((group_rows, head_count, HD), jnp.float32),
    )
    carry = absorb(start_carry, query_heads, ctx_keys, ctx_values, ctx_lift[:, None, None])
    pieces = in_one_piece((group_keys, group_values), SP, 0, 1)
    row_count = pieces[0].shape[0]
    keys = pieces[0].reshape(row_count, head_count, QK)
    values = pieces[1].reshape(row_count, head_count, HD)
    carry = absorb(carry, query_heads, keys, values, 0.0)
    highest, total, mixed = carry
    attended = (
        (mixed / jnp.transpose(total)[:, :, None])
        .astype(jnp.bfloat16)
        .reshape(group_rows, head_count * HD)
    )
    out = sent_and_summed(
        jnp.dot(attended, w_output, preferred_element_type=jnp.float32).astype(jnp.bfloat16),
        "tp",
        0,
    )
    return (latent_tokens.astype(jnp.float32) + gate_vec[0] * out).astype(jnp.bfloat16)


def solution(mesh):
    finer = Mesh(mesh.devices.reshape(8, 8, mesh.shape["tp"]), ("sp_0", "sp_1", "tp"))
    in_specs = (
        P(SP_TP, None),
        P(SP, None),
        P(),
        P(),
        P(SP, "tp"),
        P(SP, "tp"),
        P(SP, "tp"),
        P(),
        P(None, "tp"),
        P(),
        P(),
        P(),
        P(),
        P(None, None, "tp"),
        P(),
        P("tp"),
        P("tp", None),
    )
    out_specs = P(SP_TP, None)
    return jax.shard_map(local, mesh=finer, in_specs=in_specs, out_specs=out_specs, check_vma=False)
```

profile of v0, /device:TPU:1, one launch (start us, length us, event | category | flops | bytes accessed | tf_op | source)
XLA Modules:
  0.0 226.2 jit_solution(14526996260051699909)
XLA Ops:
  6.5 0.0 copy-start
  6.5 0.0 copy-start.2
  6.6 0.0 copy-start.9
  6.6 0.0 all-gather.3.cloned.1.call-start
  6.6 0.7 all-gather.3.cloned.1.call-update
  7.3 0.9 fusion.51
  8.2 0.8 fusion.53
  9.0 0.8 fusion.55
  9.9 0.8 fusion.56
  10.7 20.5 %all-reduce.1 = (f32[1,256]{1,0:T(1,128)S(1)}, f32[2,256]{1,0:T(2,128)S(1)}, f32[2,256]{1,0:T(2,128)S(1)}) all-reduce(f32[1,256]{1,0:T(1,128)S(1)} %fusion.51, f32[2,256]{1,0:T(2,128)S(1)} %fusion.55, f32[2,256]{1,0:T(2,128)S(1)} %fusion.56), channel_id=1, replica_groups=mesh['sp_0'=8,'sp_1'=8,'tp'=8] {'sp_0'}, use_global_device_ids=true, to_apply=%region_4.5 | all-reduce | flops 1280 | bytes 10240 | tf_op jit(solution)/shard_map/psum | solution.py:19
  31.2 14.8 %all-reduce = (f32[1,256]{1,0:T(1,128)S(1)}, f32[2,256]{1,0:T(2,128)S(1)}, f32[2,256]{1,0:T(2,128)S(1)}) all-reduce(f32[1,256]{1,0:T(1,128)S(1)} %get-tuple-element.8, f32[2,256]{1,0:T(2,128)S(1)} %get-tuple-element.9, f32[2,256]{1,0:T(2,128)S(1)} %get-tuple-element.10), channel_id=1, replica_groups=mesh['sp_0'=8,'sp_1'=8,'tp'=8] {'sp_1'}, use_global_device_ids=true, to_apply=%region_5.6 | all-reduce | flops 1280 | bytes 10240 | tf_op jit(solution)/shard_map/psum | solution.py:19
  46.0 20.5 %all_gather.9 = f32[5,2048]{1,0:T(8,128)S(1)} all-gather(f32[5,256]{1,0:T(8,128)S(1)} %pad_maximum_fusion.7), channel_id=1, replica_groups=mesh['sp_0'=8,'sp_1'=8,'tp'=8] {'tp'}, dimensions={1}, use_global_device_ids=true | all-gather | bytes 46080 | tf_op jit(solution)/shard_map/all_gather | solution.py:28
  66.5 1.0 fusion.29
  67.4 0.9 fusion.33
  68.4 0.8 broadcast_in_dim.13
  69.2 3.9 %all-to-all-start = ((bf16[8,16,2048]{2,1,0:T(8,128)(2,1)}), bf16[8,16,2048]{2,1,0:T(8,128)(2,1)S(1)}, u32[]{:S(2)}, u32[]{:S(2)}) async-start(bf16[8,16,2048]{2,1,0:T(8,128)(2,1)} %broadcast_in_dim.13), calls=%async_computation | async-start | bytes 1048576 | tf_op jit(solution)/shard_map/all_to_all | solution.py:33
  73.1 0.0 all-gather.5.cloned.1.call-start
  73.1 0.9 slice_bitcast_fusion
  74.0 0.1 copy.18
  74.1 0.1 broadcast_multiply_fusion.1
  74.2 0.1 fusion.45
  74.2 8.2 %all-to-all-done = bf16[8,16,2048]{2,1,0:T(8,128)(2,1)S(1)} async-done(((bf16[8,16,2048]{2,1,0:T(8,128)(2,1)}), bf16[8,16,2048]{2,1,0:T(8,128)(2,1)S(1)}, u32[]{:S(2)}, u32[]{:S(2)}) %all-to-all-start) | async-done | bytes 524320 | tf_op jit(solution)/shard_map/all_to_all | solution.py:33
  82.4 0.0 copy-done
  82.4 0.4 multiply_reduce_fusion.2
  82.8 0.0 copy-done.7
  82.9 0.2 fusion.38
  83.1 0.0 copy-done.6
  83.1 0.3 fusion.20
  83.4 0.0 copy-done.10
  83.5 0.1 multiply_multiply_fusion
  83.6 0.0 copy-done.2
  83.6 0.4 multiply_reduce_fusion.4
  84.0 0.0 copy-done.9
  84.0 0.1 multiply_multiply_fusion.1
  84.1 0.0 copy-done.5
  84.1 0.3 convolution_convert_fusion.2
  84.3 0.6 pad_maximum_fusion.2
  85.0 0.0 all-gather.5.cloned.1.call-update
  85.0 10.3 %all-gather.3.cloned.1.call-done = bf16[512,2048]{1,0:T(8,128)(2,1)} async-done(((bf16[8,2048]{1,0:T(8,128)(2,1)}), bf16[512,2048]{1,0:T(8,128)(2,1)}) %all-gather.3.cloned.1.call-update) | async-done | bytes 2097168 | tf_op jit(solution)/shard_map/all_gather | solution.py:172
  95.3 2.1 fusion.2
  97.4 0.0 copy-done.8
  97.4 0.0 copy-start.1
  97.4 2.9 %multiply_reduce_fusion = (f32[512]{0:T(512)S(1)}, f32[512,256]{0,1:T(8,128)S(1)}) fusion(bf16[2048,256]{1,0:T(8,128)(2,1)S(1)} %copy-done, bf16[512,2048]{1,0:T(8,128)(2,1)} %all-gather.3.cloned.1.call-done, f32[2048]{0:T(1024)S(1)} %bitcast.109, f32[2048]{0:T(1024)S(1)} %bitcast.111, f32[2048]{0:T(1024)S(1)} %copy-done.8, f32[512]{0:T(512)S(1)} %add_rsqrt_fusion.2), kind=kOutput, calls=%fused_computation.32 | convolution fusion | flops 543424000 | bytes 3698688 | tf_op jit(solution)/shard_map/dot_general | solution.py:95
  100.3 0.0 copy-start.11
  100.3 0.3 fusion.24
  100.6 0.0 copy-done.1
  100.6 1.0 fusion.19
  101.6 0.1 multiply_reduce_fusion.1
  101.7 0.0 copy-done.11
  101.7 0.4 fusion.66
  102.1 0.3 convolution_convert_fusion.1
  102.4 88.4 %all-gather.5.cloned.1.call-done = bf16[8192,320]{0,1:T(8,128)(2,1)} async-done(((bf16[128,320]{0,1:T(8,128)(2,1)}), bf16[8192,320]{0,1:T(8,128)(2,1)}) %all-gather.5.cloned.1.call-update) | async-done | bytes 5242896 | tf_op jit(solution)/shard_map/all_gather | solution.py:28
  190.8 1.9 slice-done
  192.7 1.4 fusion.67
  194.1 1.4 fusion
  195.5 1.6 slice-done.1
  197.1 1.7 fusion.11
  198.8 0.2 fusion.21
  199.0 0.3 fusion.18
  199.3 0.0 copy-done.4
  199.4 0.3 convolution_convert_fusion
  199.7 18.9 %all_to_all.10 = bf16[8,16,2048]{2,1,0:T(8,128)(2,1)S(1)} all-to-all(bf16[8,16,2048]{2,1,0:T(8,128)(2,1)S(1)} %bitcast.99), channel_id=1, replica_groups=mesh['sp_0'=8,'sp_1'=8,'tp'=8] {'tp'}, dimensions={0} | all-to-all | bytes 1048576 | tf_op jit(solution)/shard_map/all_to_all | solution.py:55
  218.6 0.1 convert_reduce_fusion
  218.7 0.7 fusion.34
  (30 shorter events, 0.3 us)
Async XLA Ops:
  6.5 75.9 %copy-start = (bf16[2048,256]{1,0:T(8,128)(2,1)S(1)}, bf16[2048,256]{1,0:T(8,128)(2,1)}, u32[]{:S(2)}) copy-start(bf16[2048,256]{1,0:T(8,128)(2,1)} %param.27) | copy-start | bytes 3145732
  6.5 77.5 %copy-start.5 = (bf16[2,256,128]{2,1,0:T(8,128)(2,1)S(1)}, bf16[2,256,128]{2,1,0:T(8,128)(2,1)}, u32[]{:S(2)}) copy-start(bf16[2,256,128]{2,1,0:T(8,128)(2,1)} %param.30) | copy-start | bytes 393220
  6.5 76.3 %copy-start.7 = (f32[256]{0:T(256)S(1)}, f32[256]{0:T(256)}, u32[]{:S(2)}) copy-start(f32[256]{0:T(256)} %param.29) | copy-start | bytes 3076
  6.5 76.5 %copy-start.6 = (bf16[2048,32]{0,1:T(8,128)(2,1)S(1)}, bf16[2048,32]{0,1:T(8,128)(2,1)}, u32[]{:S(2)}) copy-start(bf16[2048,32]{0,1:T(8,128)(2,1)} %param.28) | copy-start | bytes 393220
  6.5 76.9 %copy-start.10 = (f32[96]{0:T(128)S(1)}, f32[96]{0:T(128)}, u32[]{:S(2)}) copy-start(f32[96]{0:T(128)} %param.31) | copy-start | bytes 1156
  6.5 77.0 %copy-start.2 = (bf16[2048,192]{0,1:T(8,128)(2,1)S(1)}, bf16[2048,192]{0,1:T(8,128)(2,1)}, u32[]{:S(2)}) copy-start(bf16[2048,192]{0,1:T(8,128)(2,1)} %param.25) | copy-start | bytes 2359300
  6.6 77.4 %copy-start.9 = (f32[96]{0:T(128)S(1)}, f32[96]{0:T(128)}, u32[]{:S(2)}) copy-start(f32[96]{0:T(128)} %param.26) | copy-start | bytes 1156
  6.6 88.7 %all-gather.3.cloned.1.call-start = ((), (), s32[]{:S(2)}) async-start(), calls=%async_computation.2 | async-start | bytes 2129920 | tf_op jit(solution)/shard_map/all_gather | solution.py:172
  69.2 13.2 %all-to-all-start = ((bf16[8,16,2048]{2,1,0:T(8,128)(2,1)}), bf16[8,16,2048]{2,1,0:T(8,128)(2,1)S(1)}, u32[]{:S(2)}, u32[]{:S(2)}) async-start(bf16[8,16,2048]{2,1,0:T(8,128)(2,1)} %broadcast_in_dim.13), calls=%async_computation | async-start | bytes 1048576 | tf_op jit(solution)/shard_map/all_to_all | solution.py:33
  73.1 24.3 %copy-start.8 = (f32[2048]{0:T(1024)S(1)}, f32[2048]{0:T(1024)}, u32[]{:S(2)}) copy-start(f32[2048]{0:T(1024)} %param.24) | copy-start | bytes 24580
  73.1 117.7 %all-gather.5.cloned.1.call-start = ((), (), s32[]{:S(2)}) async-start(), calls=%async_computation.3 | async-start | bytes 5324800 | tf_op jit(solution)/shard_map/all_gather | solution.py:28
  97.4 3.2 %copy-start.1 = (bf16[512,2048]{1,0:T(8,128)(2,1)S(1)}, bf16[512,2048]{1,0:T(8,128)(2,1)}, u32[]{:S(2)}) copy-start(bf16[512,2048]{1,0:T(8,128)(2,1)} %all-gather.3.cloned.1.call-done) | copy-start | bytes 6291460
  100.3 1.4 copy-start.11
  190.8 1.9 slice-start
  195.5 1.6 slice-start.1
  197.1 2.3 %copy-start.4 = (bf16[128,2048]{1,0:T(8,128)(2,1)S(1)}, bf16[128,2048]{1,0:T(8,128)(2,1)}, u32[]{:S(2)}) copy-start(bf16[128,2048]{1,0:T(8,128)(2,1)} %param.33) | copy-start | bytes 1572868
  197.1 21.6 %copy-start.3 = (bf16[16,2048]{1,0:T(8,128)(2,1)S(1)}, bf16[16,2048]{1,0:T(8,128)(2,1)}, u32[]{:S(2)}) copy-start(bf16[16,2048]{1,0:T(8,128)(2,1)} %param.17) | copy-start | bytes 196612
Sparse Core Ops, SparseCore 0:
  10.4 84.8 all-gather.2
  98.3 92.4 all-gather.4
where the time goes:
time: 227 us; the launch traced here: 226 us
  waiting for transfers between devices  108 us (48%)
  blocking collectives  74.6 us (33%)
  between operations  13.7 us (6%)
  matrix products  12.7 us (6%)
  other arithmetic  8.28 us (4%)
  local copies, waits for them, and re-layouts  5.41 us (2%)
  starting transfers between devices  3.9 us (2%)
    all_gather x1, waiting for transfers between devices, in_one_piece(): lax.all_gather(both, axis, axis=dim, tiled=True)  88.4 us
    psum x2, blocking collectives, over_axes(): return functools.reduce(lax.psum, axes, value)  35.2 us
    all_gather x1, blocking collectives, in_one_piece(): lax.all_gather(both, axis, axis=dim, tiled=True)  20.5 us
    all_to_all x1, blocking collectives, sent_and_summed(): tiles = lax.all_to_all(split_up(value, dim, count), axis, 0, 0, tiled=True)  18.9 us
    all_gather x1, waiting for transfers between devices, local(): ctx_rows = lax.all_gather(context_tokens, SP, axis=0, tiled=True)  10.3 us
    all_to_all x1, waiting for transfers between devices, copy_for_each(): return lax.all_to_all(copies, axis, split_axis=0, concat_axis=0, tiled=True)  8.21 us
  transfers between devices with their start and end apart: 3, of which 3 were waited for; matrix products, arithmetic and copies ran while one was open for 7% of the time, Pallas kernels for 0%

commit v1 on v0

--- a/solution.py
+++ b/solution.py
@@ -169,7 +169,10 @@
     hidden_lat = (
         rms_normed(latent_tokens, norm_gain) * (1.0 + scale_vec[0]) + shift_vec[0]
     ).astype(jnp.bfloat16)
-    ctx_rows = lax.all_gather(context_tokens, SP, axis=0, tiled=True)
+    size = lax.axis_size(SP)
+    parts = jnp.stack([context_tokens for _ in range(size)])
+    parts = lax.all_to_all(parts, SP, split_axis=0, concat_axis=0)
+    ctx_rows = jnp.concatenate(parts, axis=0)
     ctx_hidden = (rms_normed(ctx_rows, norm_gain) * (1.0 + scale_vec[1]) + shift_vec[1]).astype(
         jnp.bfloat16
     )

time: 227 us -> 246 us (1.084)
  waiting for transfers between devices: 108 us -> 120 us
  starting transfers between devices: 3.9 us -> 9.8 us
    all_to_all x0 -> x1, waiting for transfers between devices: none -> 52.5 us  [local(): parts = lax.all_to_all(parts, SP, split_axis=0, concat_axis=0)]
    all_gather x1, waiting for transfers between devices: 88.4 us -> 59.2 us  [in_one_piece(): lax.all_gather(both, axis, axis=dim, tiled=True)]
    all_gather x1 -> x0, waiting for transfers between devices: 10.3 us -> none  [local(): ctx_rows = lax.all_gather(context_tokens, SP, axis=0, tiled=True)]
    all_to_all x0 -> x1, starting transfers between devices: none -> 5.94 us  [local(): parts = lax.all_to_all(parts, SP, split_axis=0, concat_axis=0)]
  transfers between devices with their start and end apart: 3 -> 3, of which waited for: 3 -> 3; matrix products, arithmetic and copies ran while one was open for 7% -> 3% of each run, Pallas kernels for 0% -> 0%
where the time goes in v1:
time: 246 us; the launch traced here: 245 us
  waiting for transfers between devices  120 us (49%)
  blocking collectives  74.6 us (30%)
  between operations  13.7 us (6%)
  matrix products  13 us (5%)
  starting transfers between devices  9.8 us (4%)
  local copies, waits for them, and re-layouts  7.12 us (3%)
  other arithmetic  6.78 us (3%)
    all_gather x1, waiting for transfers between devices, in_one_piece(): lax.all_gather(both, axis, axis=dim, tiled=True)  59.2 us
    all_to_all x1, waiting for transfers between devices, local(): parts = lax.all_to_all(parts, SP, split_axis=0, concat_axis=0)  52.5 us
    psum x2, blocking collectives, over_axes(): return functools.reduce(lax.psum, axes, value)  34.5 us
    all_gather x1, blocking collectives, in_one_piece(): lax.all_gather(both, axis, axis=dim, tiled=True)  21.1 us
    all_to_all x1, blocking collectives, sent_and_summed(): tiles = lax.all_to_all(split_up(value, dim, count), axis, 0, 0, tiled=True)  18.9 us
    all_to_all x1, waiting for transfers between devices, copy_for_each(): return lax.all_to_all(copies, axis, split_axis=0, concat_axis=0, tiled=True)  8.23 us
    all_to_all x1, starting transfers between devices, local(): parts = lax.all_to_all(parts, SP, split_axis=0, concat_axis=0)  5.94 us
  transfers between devices with their start and end apart: 3, of which 3 were waited for; matrix products, arithmetic and copies ran while one was open for 3% of the time, Pallas kernels for 0%

profile of v1, /device:TPU:1, one launch (start us, length us, event | category | flops | bytes accessed | tf_op | source)
XLA Modules:
  0.0 244.9 jit_solution(8070435181512765253)
XLA Ops:
  6.5 0.0 copy-start
  6.5 0.0 copy-start.5
  6.6 1.1 fusion.30
  7.6 0.9 fusion.52
  8.6 0.8 fusion.54
  9.4 0.8 fusion.56
  10.2 0.8 fusion.57
  11.0 20.5 %all-reduce.1 = (f32[1,256]{1,0:T(1,128)S(1)}, f32[2,256]{1,0:T(2,128)S(1)}, f32[2,256]{1,0:T(2,128)S(1)}) all-reduce(f32[1,256]{1,0:T(1,128)S(1)} %fusion.52, f32[2,256]{1,0:T(2,128)S(1)} %fusion.56, f32[2,256]{1,0:T(2,128)S(1)} %fusion.57), channel_id=1, replica_groups=mesh['sp_0'=8,'sp_1'=8,'tp'=8] {'sp_0'}, use_global_device_ids=true, to_apply=%region_4.5 | all-reduce | flops 1280 | bytes 10240 | tf_op jit(solution)/shard_map/psum | solution.py:19
  31.5 14.1 %all-reduce = (f32[1,256]{1,0:T(1,128)S(1)}, f32[2,256]{1,0:T(2,128)S(1)}, f32[2,256]{1,0:T(2,128)S(1)}) all-reduce(f32[1,256]{1,0:T(1,128)S(1)} %get-tuple-element.8, f32[2,256]{1,0:T(2,128)S(1)} %get-tuple-element.9, f32[2,256]{1,0:T(2,128)S(1)} %get-tuple-element.10), channel_id=1, replica_groups=mesh['sp_0'=8,'sp_1'=8,'tp'=8] {'sp_1'}, use_global_device_ids=true, to_apply=%region_5.6 | all-reduce | flops 1280 | bytes 10240 | tf_op jit(solution)/shard_map/psum | solution.py:19
  45.6 21.1 %all_gather.6 = f32[5,2048]{1,0:T(8,128)S(1)} all-gather(f32[5,256]{1,0:T(8,128)S(1)} %pad_maximum_fusion.7), channel_id=1, replica_groups=mesh['sp_0'=8,'sp_1'=8,'tp'=8] {'tp'}, dimensions={1}, use_global_device_ids=true | all-gather | bytes 46080 | tf_op jit(solution)/shard_map/all_gather | solution.py:28
  66.8 0.9 fusion.34
  67.7 0.8 broadcast_in_dim.13
  68.6 3.9 %all-to-all-start = ((bf16[8,16,2048]{2,1,0:T(8,128)(2,1)}), bf16[8,16,2048]{2,1,0:T(8,128)(2,1)S(1)}, u32[]{:S(2)}, u32[]{:S(2)}) async-start(bf16[8,16,2048]{2,1,0:T(8,128)(2,1)} %broadcast_in_dim.13), calls=%async_computation | async-start | bytes 1048576 | tf_op jit(solution)/shard_map/all_to_all | solution.py:33
  72.4 0.0 all-gather.2.cloned.1.call-start
  72.4 0.8 slice_bitcast_fusion
  73.3 0.1 copy.22
  73.4 0.1 broadcast_multiply_fusion.1
  73.5 0.1 fusion.46
  73.6 8.2 %all-to-all-done = bf16[8,16,2048]{2,1,0:T(8,128)(2,1)S(1)} async-done(((bf16[8,16,2048]{2,1,0:T(8,128)(2,1)}), bf16[8,16,2048]{2,1,0:T(8,128)(2,1)S(1)}, u32[]{:S(2)}, u32[]{:S(2)}) %all-to-all-start) | async-done | bytes 524320 | tf_op jit(solution)/shard_map/all_to_all | solution.py:33
  81.8 1.5 multiply_reduce_fusion.4
  83.3 1.2 fusion.21
  84.5 0.0 copy-done
  84.5 0.4 multiply_reduce_fusion.2
  84.9 0.0 copy-done.3
  84.9 0.0 copy-done.6
  84.9 0.2 convolution_convert_fusion.2
  85.2 0.2 fusion.39
  85.5 0.0 copy-done.9
  85.5 0.1 multiply_multiply_fusion
  85.6 0.0 copy-done.8
  85.6 0.1 multiply_multiply_fusion.1
  85.7 0.6 pad_maximum_fusion.2
  86.4 0.0 all-gather.2.cloned.1.call-update
  86.4 0.0 copy-done.5
  86.4 0.0 copy-start.7
  86.4 1.6 stack.11
  88.0 5.9 %all-to-all-start.1 = ((bf16[64,8,2048]{2,1,0:T(8,128)(2,1)}), bf16[64,8,2048]{2,1,0:T(8,128)(2,1)S(1)}, u32[]{:S(2)}, u32[]{:S(2)}) async-start(bf16[64,8,2048]{2,1,0:T(8,128)(2,1)} %stack.11), calls=%async_computation.1 | async-start | bytes 4194304 | tf_op jit(solution)/shard_map/all_to_all | solution.py:174
  94.0 52.5 %all-to-all-done.1 = bf16[64,8,2048]{2,1,0:T(8,128)(2,1)S(1)} async-done(((bf16[64,8,2048]{2,1,0:T(8,128)(2,1)}), bf16[64,8,2048]{2,1,0:T(8,128)(2,1)S(1)}, u32[]{:S(2)}, u32[]{:S(2)}) %all-to-all-start.1) | async-done | bytes 2097184 | tf_op jit(solution)/shard_map/all_to_all | solution.py:174
  146.5 0.5 fusion.7
  147.0 0.1 rsqrt.62
  147.1 0.0 copy-done.7
  147.1 0.0 copy-start.4
  147.1 1.2 multiply_reduce_fusion
  148.3 0.0 copy-start.10
  148.3 0.3 fusion.25
  148.6 0.0 copy-done.4
  148.6 1.0 fusion.20
  149.6 0.1 multiply_reduce_fusion.1
  149.6 0.0 copy-done.10
  149.7 0.4 fusion.67
  150.0 0.3 convolution_convert_fusion.1
  150.3 59.2 %all-gather.2.cloned.1.call-done = bf16[8192,320]{0,1:T(8,128)(2,1)} async-done(((bf16[128,320]{0,1:T(8,128)(2,1)}), bf16[8192,320]{0,1:T(8,128)(2,1)}) %all-gather.2.cloned.1.call-update) | async-done | bytes 5242896 | tf_op jit(solution)/shard_map/all_gather | solution.py:28
  209.5 1.9 slice-done
  211.4 1.4 fusion.68
  212.8 1.4 fusion
  214.2 1.6 slice-done.1
  215.8 1.7 fusion.12
  217.5 0.2 fusion.22
  217.8 0.3 fusion.19
  218.1 0.0 copy-done.2
  218.1 0.3 convolution_convert_fusion
  218.4 18.9 %all_to_all.15 = bf16[8,16,2048]{2,1,0:T(8,128)(2,1)S(1)} all-to-all(bf16[8,16,2048]{2,1,0:T(8,128)(2,1)S(1)} %bitcast.115), channel_id=1, replica_groups=mesh['sp_0'=8,'sp_1'=8,'tp'=8] {'tp'}, dimensions={0} | all-to-all | bytes 1048576 | tf_op jit(solution)/shard_map/all_to_all | solution.py:55
  237.3 0.1 convert_reduce_fusion
  237.4 0.7 fusion.35
  (29 shorter events, 0.3 us)
Async XLA Ops:
  6.5 78.0 %copy-start = (bf16[2048,256]{1,0:T(8,128)(2,1)S(1)}, bf16[2048,256]{1,0:T(8,128)(2,1)}, u32[]{:S(2)}) copy-start(bf16[2048,256]{1,0:T(8,128)(2,1)} %param.27) | copy-start | bytes 3145732
  6.5 78.4 %copy-start.3 = (bf16[2,256,128]{2,1,0:T(8,128)(2,1)S(1)}, bf16[2,256,128]{2,1,0:T(8,128)(2,1)}, u32[]{:S(2)}) copy-start(bf16[2,256,128]{2,1,0:T(8,128)(2,1)} %param.30) | copy-start | bytes 393220
  6.5 78.4 %copy-start.6 = (f32[256]{0:T(256)S(1)}, f32[256]{0:T(256)}, u32[]{:S(2)}) copy-start(f32[256]{0:T(256)} %param.29) | copy-start | bytes 3076
  6.5 78.9 %copy-start.9 = (f32[96]{0:T(128)S(1)}, f32[96]{0:T(128)}, u32[]{:S(2)}) copy-start(f32[96]{0:T(128)} %param.31) | copy-start | bytes 1156
  6.5 79.1 %copy-start.8 = (f32[96]{0:T(128)S(1)}, f32[96]{0:T(128)}, u32[]{:S(2)}) copy-start(f32[96]{0:T(128)} %param.26) | copy-start | bytes 1156
  6.5 79.8 %copy-start.5 = (bf16[8,2048]{1,0:T(8,128)(2,1)S(1)}, bf16[8,2048]{1,0:T(8,128)(2,1)}, u32[]{:S(2)}) copy-start(bf16[8,2048]{1,0:T(8,128)(2,1)} %param.18) | copy-start | bytes 98308
  68.6 13.2 %all-to-all-start = ((bf16[8,16,2048]{2,1,0:T(8,128)(2,1)}), bf16[8,16,2048]{2,1,0:T(8,128)(2,1)S(1)}, u32[]{:S(2)}, u32[]{:S(2)}) async-start(bf16[8,16,2048]{2,1,0:T(8,128)(2,1)} %broadcast_in_dim.13), calls=%async_computation | async-start | bytes 1048576 | tf_op jit(solution)/shard_map/all_to_all | solution.py:33
  72.4 137.1 %all-gather.2.cloned.1.call-start = ((), (), s32[]{:S(2)}) async-start(), calls=%async_computation.3 | async-start | bytes 5324800 | tf_op jit(solution)/shard_map/all_gather | solution.py:28
  86.4 60.7 %copy-start.7 = (f32[2048]{0:T(1024)S(1)}, f32[2048]{0:T(1024)}, u32[]{:S(2)}) copy-start(f32[2048]{0:T(1024)} %param.24) | copy-start | bytes 24580
  88.0 58.4 %all-to-all-start.1 = ((bf16[64,8,2048]{2,1,0:T(8,128)(2,1)}), bf16[64,8,2048]{2,1,0:T(8,128)(2,1)S(1)}, u32[]{:S(2)}, u32[]{:S(2)}) async-start(bf16[64,8,2048]{2,1,0:T(8,128)(2,1)} %stack.11), calls=%async_computation.1 | async-start | bytes 4194304 | tf_op jit(solution)/shard_map/all_to_all | solution.py:174
  147.1 1.5 copy-start.4
  148.3 1.4 copy-start.10
  209.5 1.9 slice-start
  214.2 1.6 slice-start.1
  215.8 2.3 copy-start.2
  215.8 21.6 %copy-start.1 = (bf16[16,2048]{1,0:T(8,128)(2,1)S(1)}, bf16[16,2048]{1,0:T(8,128)(2,1)}, u32[]{:S(2)}) copy-start(bf16[16,2048]{1,0:T(8,128)(2,1)} %param.17) | copy-start | bytes 196612
Sparse Core Ops, SparseCore 0:
  86.5 122.9 all-gather.1
